TPU v7x, 32 devices: a whole 2x2x4 slice. The times are simulated.
32 devices in a mesh: ep: 8 (over z, y), tp: 4 (over x, core).
Axes of the slice: x: 2, y: 2, z: 4, core: 2. Of those that a mesh axis runs over, the one named last changes fastest.
Arguments:
- query_rows: bfloat16 [3072, 1024], P('ep', 'tp'), may hold values from -6 to 6
- key_rows: bfloat16 [3072, 512], P('ep', 'tp'), may hold values from -6 to 6
- value_rows: bfloat16 [3072, 512], P('ep', 'tp'), may hold values from -6 to 6
- break_bias: bfloat16 [3072, 16], P('ep', 'tp'), may hold values from -14 to 0
- mixer_weight: bfloat16 [1024, 2048], P('tp'), may hold values from -0.1875 to 0.1875
- mixer_gain: bfloat16 [2048], replicated, may hold values from 0.099609375 to 1.8984375
- expert_input: bfloat16 [4096, 2048], P(('ep', 'tp')), may hold values from -6 to 6
- expert_gain: bfloat16 [2048], replicated, may hold values from 0.099609375 to 1.8984375
- route_ids: int32 [4096, 2], P('ep'), may hold values from 0 to 15, all different within a row; in each aligned block of 128 rows (0 to 127, 128 to 255, ...) at most 32 rows name the same one
- route_weights: float32 [4096, 2], P(('ep', 'tp')), may hold values from 0.2 to 2
- expert_gate: bfloat16 [16, 2048, 2048], P('ep', None, 'tp'), may hold values from -0.125 to 0.125
- expert_up: bfloat16 [16, 2048, 2048], P('ep', None, 'tp'), may hold values from -0.125 to 0.125
- expert_down: bfloat16 [16, 2048, 2048], P('ep', 'tp'), may hold values from -0.125 to 0.125
- shared_gate: bfloat16 [2048, 512], replicated, may hold values from -0.125 to 0.125
- shared_up: bfloat16 [2048, 512], replicated, may hold values from -0.125 to 0.125
- shared_down: bfloat16 [512, 2048], replicated, may hold values from -0.25 to 0.25
Outputs:
- mixer_out: bfloat16 [3072, 2048], P(('ep', 'tp'))
- expert_out: bfloat16 [4096, 2048], P(('ep', 'tp'))
Inputs may be any that keep to these rules, and one draw needn't show every extreme that they name: `route_ids`: each row names 2 different experts. Within the rows of one device no expert is named more than 32 times, and in every draw some expert is named exactly 32 times within the rows of some device.
All inputs are finite; a program needn't handle non-finite values.
Results may differ from a plain program's by a relative error of at most 0.012.
Values may be sent and summed in bfloat16 or wider, within the bound.
A program may use at most 192 MiB of HBM per device.

v0:
```python
import functools

import jax
import jax.numpy as jnp
from jax import lax
from jax.experimental import pallas as pl
from jax.experimental.pallas import tpu as pltpu
from jax.sharding import PartitionSpec as P

DH = 64
TOPK = 2
SEQS = 1
MESH = pl.DeviceIdType.MESH

norm_eps = 1e-06
F32 = jnp.float32
BF16 = jnp.bfloat16


def dot(left, right):
    return jnp.dot(left, right, preferred_element_type=F32)


def iota(shape, dim):
    return lax.broadcasted_iota(jnp.int32, shape, dim)


def joined(values):
    rows = values.shape[-2]
    flat = (-1, values.shape[-1])
    if rows % 16:
        return values.astype(F32).reshape(flat).astype(BF16)
    return values.reshape(flat)


def layer_kernel(
    cfg,
    query_ref,
    key_ref,
    value_ref,
    bias_ref,
    mixer_gain_ref,
    input_ref,
    expert_gain_ref,
    ids_ref,
    route_ref,
    mixer_hbm,
    gate_hbm,
    up_hbm,
    down_hbm,
    shared_gate_hbm,
    shared_up_hbm,
    shared_down_hbm,
    mixer_out_ref,
    expert_out_ref,
    arrived,
    outgoing,
    partial,
    from_core,
    from_x,
    returned,
    gate,
    up,
    down,
    shared_gate,
    shared_up,
    shared_down,
    mixer,
    kv,
    projected,
    mixer_core,
    mixer_x,
    output,
    later,
    queries,
    normed,
    mixing,
    shared_out,
    weight_sem,
    kv_recv,
    kv_chain,
    kv_pair,
    arrive_sem,
    send_sem,
    x_sem,
    core_sem,
    core2_sem,
    s1_sem,
    r1_sem,
    s2_sem,
    r2_sem,
    s3_sem,
    r3_sem,
    mixer_sem,
):
    ep_size, experts_local, capacity, heads, kv_heads = cfg
    group = lax.axis_index("ep").astype(jnp.int32)
    tp = lax.axis_index("tp").astype(jnp.int32)
    rows, kv_width = key_ref.shape
    tokens, width = input_ref.shape
    experts = experts_local * ep_size
    groups = heads // kv_heads
    span = ep_size // SEQS

    core_of, x_of = tp % 2, tp // 2
    core_peer = tp + 1 - 2 * core_of
    x_peer = x_of * -2 + core_of + 2
    mine = core_of * 2 + x_of
    slot_core = (1 - core_of) * 2 + x_of
    slot_x = core_of * 2 + 1 - x_of
    slot_diagonal = (1 - core_of) * 2 + 1 - x_of

    place = group % span
    base = group - place
    pair_of, chain_of = place % 2, place // 2
    pair = group + 1 - 2 * pair_of
    chains = span // 2
    above = jnp.where(chain_of + 1 < chains, group + 2, group)

    def remote(source, target, sent, received, ep, to):
        return pltpu.make_async_remote_copy(
            src_ref=source,
            dst_ref=target,
            send_sem=sent,
            recv_sem=received,
            device_id=(ep, to),
            device_id_type=MESH,
        )

    barrier = pltpu.get_barrier_semaphore()

    def greet(step, carry):
        other = (group + 1 + step) % ep_size
        pl.semaphore_signal(barrier, inc=1, device_id=(other, tp), device_id_type=MESH)
        return carry

    lax.fori_loop(0, ep_size - 1, greet, 0)
    for to in (core_peer, x_peer):
        pl.semaphore_signal(barrier, inc=1, device_id=(group, to), device_id_type=MESH)

    loads = []
    for source, target in (
        (mixer_hbm, mixer),
        (gate_hbm, gate),
        (up_hbm, up),
        (down_hbm, down),
        (shared_gate_hbm, shared_gate),
        (shared_up_hbm, shared_up),
        (shared_down_hbm, shared_down),
    ):
        load = pltpu.make_async_copy(source, target, weight_sem.at[len(loads)])
        load.start()
        loads.append(load)

    parts = -(-rows // (2 * kv_width))
    kv[group, 0:rows, 0:kv_width] = key_ref[...]
    kv[group, 0:rows, kv_width : 2 * kv_width] = value_ref[...]
    biases = jnp.concatenate([bias_ref[...].astype(F32), jnp.zeros((8 - heads, rows), F32)], axis=0)
    pieces = []
    for part in range(parts):
        piece = biases[:, part * 2 * kv_width : min(rows, (part + 1) * 2 * kv_width)]
        missing = 2 * kv_width - piece.shape[1]
        if missing:
            piece = jnp.concatenate([piece, jnp.zeros((8, missing), F32)], axis=1)
        pieces.append(piece)
    while len(pieces) % 2:
        pieces.append(jnp.zeros((8, 2 * kv_width), F32))
    kv[group, rows : rows + 8 * len(pieces), :] = jnp.concatenate(pieces, axis=0).astype(BF16)

    first_token = pl.multiple_of(tp * tokens, tokens)
    first_id = ids_ref[0:1, pl.ds(first_token, tokens)]
    second_id = ids_ref[1:2, pl.ds(first_token, tokens)]
    number = iota((experts, tokens), 0)
    is_first, is_second = number == first_id, number == second_id
    named = jnp.where(is_first | is_second, 1.0, 0.0).astype(BF16)
    weight = jnp.where(is_first, route_ref[0:1, :], jnp.where(is_second, route_ref[1:2, :], 0.0))
    earlier = (iota((tokens, tokens), 0) < iota((tokens, tokens), 1)).astype(F32).astype(BF16)
    before = dot(named, earlier).astype(BF16)
    slots = experts * capacity
    slot = iota((slots, experts), 0)
    owner = iota((slots, experts), 1) * capacity
    spread = ((slot >= owner) & (slot < owner + capacity)).astype(F32).astype(BF16)
    rank = (iota((slots, tokens), 0) % capacity).astype(F32)
    chosen = (dot(spread, named) > 0.5) & (dot(spread, before) == rank)
    mixing[...] = jnp.where(chosen, dot(spread, weight.astype(BF16)), 0.0).astype(BF16)
    chosen = jnp.where(chosen, 1.0, 0.0).astype(BF16)

    values = input_ref[...].astype(F32)
    scale = lax.rsqrt(jnp.mean(values * values, axis=-1, keepdims=True) + norm_eps)
    normed[...] = (values * scale * expert_gain_ref[...].astype(F32)).astype(BF16)
    tile = min(width, 512)
    for start in range(0, width, tile):
        block = dot(chosen, normed[:, start : start + tile])
        block = block.reshape(ep_size, experts_local, capacity, tile)
        outgoing[:, :, :, start : start + tile] = block.astype(BF16)
    arrived[mine, group] = outgoing[group]

    select = {}
    for head in range(heads):
        shape = (heads * DH, kv_width)
        inside = iota(shape, 1) - (head // groups) * DH
        picked = (iota(shape, 0) - head * DH == inside) & (inside >= 0) & (inside < DH)
        select[head] = picked.astype(F32)
        queries[head] = dot(query_ref[...], (select[head] * DH ** (-0.5)).astype(BF16)).astype(BF16)

    pl.semaphore_wait(barrier, ep_size + 1)

    def chain_copy(step):
        block = base + jnp.maximum(place - 2 * step, 0)
        return remote(kv.at[block], kv.at[block], kv_chain.at[step], kv_recv.at[block], above, tp)

    def pair_copy(step):
        block = base + jnp.maximum(place - 2 * step, 0)
        return remote(kv.at[block], kv.at[block], kv_pair.at[step], kv_recv.at[block], pair, tp)

    def await_kv(block):
        remote(kv.at[block], kv.at[block], kv_chain.at[0], kv_recv.at[block], pair, tp).wait_recv()

    @pl.when(chain_of + 1 < chains)
    def _():
        chain_copy(0).start()

    @pl.when(pair_of == 0)
    def _():
        pair_copy(0).start()

    def dispatch_copy(step):
        to = (group + ep_size - 1 - step) % ep_size
        return remote(
            outgoing.at[to], arrived.at[mine, group], send_sem.at[to], arrive_sem.at[mine, group], to, tp
        )

    def dispatch(step, carry):
        dispatch_copy(step).start()
        return carry

    def x_copy(source, block):
        return remote(source, arrived.at[mine, block], x_sem.at[block], arrive_sem.at[mine, block], group, x_peer)

    def core_copy(source, block):
        return remote(
            source, arrived.at[mine, block], core_sem.at[block], arrive_sem.at[mine, block], group, core_peer
        )

    def core2_copy(block):
        part = arrived.at[slot_x, block]
        return remote(part, part, core2_sem.at[block], arrive_sem.at[slot_x, block], group, core_peer)

    def await_rows(place_of, block):
        part = arrived.at[place_of, block]
        remote(part, part, core_sem.at[block], arrive_sem.at[place_of, block], group, x_peer).wait_recv()

    x_copy(outgoing.at[group], group).start()
    core_copy(outgoing.at[group], group).start()
    lax.fori_loop(0, group, dispatch, 0)

    @pl.when(chain_of == 0)
    def _():
        lax.fori_loop(group, ep_size - 1, dispatch, 0)

    row_of = iota((rows, rows), 0)
    column_of = iota((rows, rows), 1)
    after = (column_of < row_of).astype(F32).astype(BF16)

    def visit(block, head, diagonal):
        keys = kv[block, 0:rows, 0:kv_width]
        scores = lax.dot_general(
            queries[head], keys, (((1,), (1,)), ((), ())), preferred_element_type=F32
        )
        tail = kv[block, rows : rows + 8 * len(pieces), :].astype(F32)
        bias = []
        for part in range(parts):
            line = jnp.where(iota(tail.shape, 0) == head + 8 * part, tail, 0.0)
            line = jnp.sum(line, axis=0, keepdims=True)
            bias.append(line[:, : min(2 * kv_width, rows - part * 2 * kv_width)])
        scores = scores + jnp.concatenate(bias, axis=1)
        soft = jnp.log(1.0 + jnp.exp(-jnp.abs(scores)))
        keep = -(jnp.maximum(scores, 0.0) + soft)
        if diagonal:
            keep = jnp.where(column_of < row_of, keep, 0.0)
        high = keep.astype(BF16)
        low = (keep - high.astype(F32)).astype(BF16)
        beyond = dot(high, after) + dot(low, after)
        weights = jnp.exp(jnp.minimum(scores, 0.0) - soft + beyond)
        if diagonal:
            weights = jnp.where(column_of < row_of, weights, 0.0)
        total = beyond[:, 0:1] + keep[:, 0:1]
        summed = dot(weights.astype(BF16), kv[block, 0:rows, kv_width : 2 * kv_width])
        return summed, total

    def first_visit(head, carry):
        summed, total = visit(group, head, True)
        output[head] = summed
        later[head] = total
        return carry

    lax.fori_loop(0, heads, first_visit, 0)

    def attend(step, carry):
        @pl.when(step <= chain_of)
        def _():
            await_kv(base + jnp.maximum(place - 2 * step, 0))

            @pl.when(chain_of + 1 < chains)
            def _():
                chain_copy(step).start()

            pair_copy(step).start()

        @pl.when(step == chain_of)
        def _():
            lax.fori_loop(group, ep_size - 1, dispatch, 0)

        @pl.when(step <= place)
        def _():
            block = base + jnp.maximum(place - step, 0)

            @pl.when(step % 2 == 1)
            def _():
                await_kv(block)

            def next_visit(head, carry):
                summed, total = visit(block, head, False)
                passed = later[head]
                output[head] = output[head] + jnp.exp(passed) * summed
                later[head] = passed + total
                return carry

            lax.fori_loop(0, heads, next_visit, 0)

        block = (group + step) % ep_size
        await_rows(mine, block)
        x_copy(arrived.at[mine, block], block).start()
        core_copy(arrived.at[mine, block], block).start()
        return carry

    lax.fori_loop(1, ep_size, attend, 0)

    def forward(step):
        block = (group + 1 + step) % ep_size
        await_rows(slot_x, block)
        core2_copy(block).start()

    forward(0)

    attended = jnp.zeros((rows, heads * DH), F32)
    for head in range(heads):
        attended = attended + lax.dot_general(
            output[head].astype(BF16),
            select[head].astype(BF16),
            (((1,), (1,)), ((), ())),
            preferred_element_type=F32,
        )
    attended = attended.astype(BF16)
    for load in loads:
        load.wait()
    share = projected.shape[1]
    for to in range(projected.shape[0]):
        for start in range(0, width, tile):
            block = dot(attended[to * share : (to + 1) * share], mixer[:, start : start + tile])
            projected[(to % 2) * 2 + to // 2, :, start : start + tile] = block.astype(BF16)

    mixer_core_copy = remote(
        projected.at[pl.ds((1 - core_of) * 2, 2)], mixer_core, mixer_sem.at[0], mixer_sem.at[1], group, core_peer
    )
    mixer_x_copy = remote(
        projected.at[slot_x], mixer_x, mixer_sem.at[2], mixer_sem.at[3], group, x_peer
    )
    mixer_core_copy.start()

    def core_sum_copy(step):
        return remote(
            partial.at[step, pl.ds((1 - core_of) * 2, 2)],
            from_core.at[step],
            s1_sem.at[step],
            r1_sem.at[step],
            group,
            core_peer,
        )

    def x_sum_copy(step):
        return remote(
            partial.at[step, slot_x], from_x.at[step], s2_sem.at[step], r2_sem.at[step], group, x_peer
        )

    def return_copy(step):
        to = (group + 1 + step) % ep_size
        return remote(
            partial.at[step, mine], returned.at[group], s3_sem.at[to], r3_sem.at[group], to, tp
        )

    def work(step, carry):
        @pl.when(step < ep_size)
        def _():
            @pl.when(step + 1 < ep_size)
            def _():
                forward(step + 1)

            block = (group + 1 + step) % ep_size
            await_rows(slot_core, block)
            await_rows(slot_diagonal, block)
            for expert in range(experts_local):
                piece = joined(arrived[:, block, expert])
                gate_proj = dot(piece, gate[expert])
                up_proj = dot(piece, up[expert])
                hidden = (jax.nn.silu(gate_proj) * up_proj).astype(BF16)
                for start in range(0, width, tile):
                    part = dot(hidden, down[expert, :, start : start + tile])
                    part = part.reshape(4, capacity, tile).astype(BF16)
                    partial[step, :, expert, :, start : start + tile] = part
            core_sum_copy(step).start()

        @pl.when((step >= 1) & (step <= ep_size))
        def _():
            past = step - 1
            core_sum_copy(past).wait_recv()
            for slot_of, x_at in ((slot_x, 1 - x_of), (mine, x_of)):
                for expert in range(experts_local):
                    total = partial[past, slot_of, expert].astype(F32) + from_core[
                        past, x_at, expert
                    ].astype(F32)
                    partial[past, slot_of, expert] = total.astype(BF16)
            x_sum_copy(past).start()

        @pl.when(step == ep_size - 1)
        def _():
            mixer_core_copy.wait_recv()
            for slot_of, x_at in ((slot_x, 1 - x_of), (mine, x_of)):
                total = projected[slot_of].astype(F32) + mixer_core[x_at].astype(F32)
                projected[slot_of] = total.astype(BF16)
            mixer_x_copy.start()
            gate_proj = dot(normed[...], shared_gate[...])
            up_proj = dot(normed[...], shared_up[...])
            hidden = (jax.nn.silu(gate_proj) * up_proj).astype(BF16)
            for start in range(0, width, tile):
                shared_out[:, start : start + tile] = dot(hidden, shared_down[:, start : start + tile])

        @pl.when(step >= 2)
        def _():
            past = step - 2
            x_sum_copy(past).wait_recv()
            for expert in range(experts_local):
                total = partial[past, mine, expert].astype(F32) + from_x[past, expert].astype(F32)
                partial[past, mine, expert] = total.astype(BF16)

            @pl.when(past < ep_size - 1)
            def _():
                return_copy(past).start()

        return carry

    lax.fori_loop(0, ep_size + 2, work, 0)
    returned[group] = partial[ep_size - 1, mine]

    mixer_x_copy.wait_recv()
    total = projected[mine].astype(F32) + mixer_x[...].astype(F32)
    scale = lax.rsqrt(jnp.mean(total * total, axis=-1, keepdims=True) + norm_eps)
    mixer_out_ref[...] = (total * scale * mixer_gain_ref[...].astype(F32)).astype(BF16)

    def await_return(step, carry):
        block = (group + 1 + step) % ep_size
        remote(
            returned.at[block], returned.at[block], s3_sem.at[block], r3_sem.at[block], block, tp
        ).wait_recv()
        return carry

    lax.fori_loop(0, ep_size - 1, await_return, 0)
    for start in range(0, width, tile):
        results = joined(returned[:, :, :, start : start + tile])
        mixed = lax.dot_general(
            mixing[...], results, (((0,), (0,)), ((), ())), preferred_element_type=F32
        )
        expert_out_ref[:, start : start + tile] = (
            mixed + shared_out[:, start : start + tile]
        ).astype(BF16)

    @pl.when(chain_of + 1 < chains)
    def _():
        def done(step, carry):
            chain_copy(step).wait_send()
            return carry

        lax.fori_loop(0, chain_of + 1, done, 0)

    @pl.when(pair_of == 0)
    def _():
        pair_copy(0).wait_send()

    def pair_done(step, carry):
        pair_copy(step).wait_send()
        return carry

    lax.fori_loop(1, chain_of + 1, pair_done, 0)

    def sent(step, carry):
        dispatch_copy(step).wait_send()
        return_copy(step).wait_send()
        return carry

    lax.fori_loop(0, ep_size - 1, sent, 0)

    def forwarded(block, carry):
        x_copy(arrived.at[mine, block], block).wait_send()
        core_copy(arrived.at[mine, block], block).wait_send()
        core2_copy(block).wait_send()
        core_sum_copy(block).wait_send()
        x_sum_copy(block).wait_send()
        return carry

    lax.fori_loop(0, ep_size, forwarded, 0)
    mixer_core_copy.wait_send()
    mixer_x_copy.wait_send()


def on_device(
    query_rows,
    key_rows,
    value_rows,
    break_bias,
    mixer_weight,
    mixer_gain,
    expert_input,
    expert_gain,
    route_ids,
    route_weights,
    expert_gate,
    expert_up,
    expert_down,
    shared_gate,
    shared_up,
    shared_down,
):
    rows = query_rows.shape[0]
    heads = query_rows.shape[1] // DH
    kv_width = key_rows.shape[1]
    kv_heads = kv_width // DH
    ep_size = lax.axis_size("ep")
    tp_size = lax.axis_size("tp")
    tokens, width = expert_input.shape
    experts_local, _, hidden = expert_gate.shape
    capacity = 2 * tokens * TOPK // (experts_local * ep_size)
    slots = experts_local * ep_size * capacity
    parts = -(-rows // (2 * kv_width))
    block_rows = rows + 8 * (parts + parts % 2)
    share = rows // tp_size
    cfg = (ep_size, experts_local, capacity, heads, kv_heads)
    piece = (experts_local, capacity, width)
    vmem = pl.BlockSpec(memory_space=pltpu.VMEM)
    hbm = pl.BlockSpec(memory_space=pl.ANY)
    dma = pltpu.SemaphoreType.DMA
    return pl.pallas_call(
        functools.partial(layer_kernel, cfg),
        out_shape=(
            jax.ShapeDtypeStruct((share, width), BF16),
            jax.ShapeDtypeStruct((tokens, width), BF16),
        ),
        in_specs=[vmem] * 9 + [hbm] * 7,
        out_specs=(vmem, vmem),
        scratch_shapes=[
            pltpu.VMEM((tp_size, ep_size) + piece, BF16),
            pltpu.VMEM((ep_size,) + piece, BF16),
            pltpu.VMEM((ep_size, tp_size) + piece, BF16),
            pltpu.VMEM((ep_size, 2) + piece, BF16),
            pltpu.VMEM((ep_size,) + piece, BF16),
            pltpu.VMEM((ep_size,) + piece, BF16),
            pltpu.VMEM(expert_gate.shape, BF16),
            pltpu.VMEM(expert_up.shape, BF16),
            pltpu.VMEM(expert_down.shape, BF16),
            pltpu.VMEM(shared_gate.shape, BF16),
            pltpu.VMEM(shared_up.shape, BF16),
            pltpu.VMEM(shared_down.shape, BF16),
            pltpu.VMEM(mixer_weight.shape, BF16),
            pltpu.VMEM((ep_size, block_rows, 2 * kv_width), BF16),
            pltpu.VMEM((tp_size, share, width), BF16),
            pltpu.VMEM((2, share, width), BF16),
            pltpu.VMEM((share, width), BF16),
            pltpu.VMEM((heads, rows, kv_width), F32),
            pltpu.VMEM((heads, rows, 1), F32),
            pltpu.VMEM((heads, rows, kv_width), BF16),
            pltpu.VMEM((tokens, width), BF16),
            pltpu.VMEM((slots, tokens), BF16),
            pltpu.VMEM((tokens, width), F32),
            dma((7,)),
            dma((ep_size,)),
            dma((ep_size,)),
            dma((ep_size,)),
            dma((tp_size, ep_size)),
            dma((ep_size,)),
            dma((ep_size,)),
            dma((ep_size,)),
            dma((ep_size,)),
            dma((ep_size,)),
            dma((ep_size,)),
            dma((ep_size,)),
            dma((ep_size,)),
            dma((ep_size,)),
            dma((ep_size,)),
            dma((4,)),
        ],
        compiler_params=pltpu.CompilerParams(
            collective_id=0, has_side_effects=True, vmem_limit_bytes=67043328
        ),
        name="layer",
    )(
        query_rows,
        key_rows,
        value_rows,
        break_bias.T,
        mixer_gain.reshape(1, -1),
        expert_input,
        expert_gain.reshape(1, -1),
        route_ids.T,
        route_weights.T,
        mixer_weight,
        expert_gate,
        expert_up,
        expert_down,
        shared_gate,
        shared_up,
        shared_down,
    )


def solution(mesh):
    return jax.shard_map(
        on_device,
        mesh=mesh,
        in_specs=(
            P("ep", "tp"),
            P("ep", "tp"),
            P("ep", "tp"),
            P("ep", "tp"),
            P("tp", None),
            P(),
            P(("ep", "tp"), None),
            P(),
            P("ep", None),
            P(("ep", "tp"), None),
            P("ep", None, "tp"),
            P("ep", None, "tp"),
            P("ep", "tp", None),
            P(),
            P(),
            P(),
        ),
        out_specs=(P(("ep", "tp"), None), P(("ep", "tp"), None)),
        check_vma=False,
    )
```

profile of v0, /device:TPU:12, one launch (start us, length us, event | category | flops | bytes accessed | tf_op | source)
XLA Modules:
  0.0 155.7 jit_solution(7420450570033798872)
XLA Ops:
  0.6 1.3 reshape.10.mixer_gain_ref
  1.9 1.3 reshape.11.expert_gain_ref
  3.2 148.8 %layer.1 = (bf16[96,2048]{1,0:T(8,128)(2,1)}, bf16[128,2048]{1,0:T(8,128)(2,1)}) custom-call(bf16[384,256]{1,0:T(8,128)(2,1)} %query_ref.1, bf16[384,128]{1,0:T(8,128)(2,1)} %key_ref.1, bf16[384,128]{1,0:T(8,128)(2,1)} %value_ref.1, bf16[4,384]{1,0:T(4,128)(2,1)} %bitcast.4, bf16[1,2048]{1,0:T(2,128)(2,1)} %reshape.10.mixer_gain_ref, ...), custom_call_target="tpu_custom_call" | custom-call | tf_op jit(solution)/shard_map/layer/pallas_call | solution.py:551
  152.1 1.8 %copy.20 = bf16[96,2048]{1,0:T(8,128)(2,1)} copy(bf16[96,2048]{1,0:T(8,128)(2,1)} %get-tuple-element.4) | data formatting | bytes 786432
  153.8 1.9 %copy.21 = bf16[128,2048]{1,0:T(8,128)(2,1)} copy(bf16[128,2048]{1,0:T(8,128)(2,1)} %get-tuple-element.5) | data formatting | bytes 1048576
where the time goes:
time: 156 us
  Pallas kernels  149 us (96%)
  local copies, waits for them, and re-layouts  6.23 us (4%)
    pallas_call x1, Pallas kernels, on_device(): pl.pallas_call(functools.partial(layer_kernel, cfg), out_shape=(jax.Shape...  149 us
    unnamed x2, local copies, waits for them, and re-layouts  3.65 us

commit v1 on v0

--- a/solution.py
+++ b/solution.py
@@ -23,6 +23,11 @@
 
 def iota(shape, dim):
     return lax.broadcasted_iota(jnp.int32, shape, dim)
+
+
+def as_row(ref):
+    values = ref[...].astype(F32)
+    return jnp.concatenate([values[at : at + 1] for at in range(values.shape[0])], axis=1)
 
 
 def joined(values):
@@ -54,7 +59,9 @@
     mixer_out_ref,
     expert_out_ref,
     arrived,
-    outgoing,
+    raw,
+    info,
+    crossing,
     partial,
     from_core,
     from_x,
@@ -81,7 +88,13 @@
     kv_chain,
     kv_pair,
     arrive_sem,
-    send_sem,
+    raw_recv,
+    raw_up,
+    raw_down,
+    info_recv,
+    info_up,
+    info_down,
+    y_sem,
     x_sem,
     core_sem,
     core2_sem,
@@ -116,6 +129,9 @@
     pair = group + 1 - 2 * pair_of
     chains = span // 2
     above = jnp.where(chain_of + 1 < chains, group + 2, group)
+    line, lines = group // 2, ep_size // 2
+    upper = jnp.where(line + 1 < lines, group + 2, group)
+    lower = jnp.where(line > 0, group - 2, group)
 
     def remote(source, target, sent, received, ep, to):
         return pltpu.make_async_remote_copy(
@@ -175,25 +191,44 @@
     named = jnp.where(is_first | is_second, 1.0, 0.0).astype(BF16)
     weight = jnp.where(is_first, route_ref[0:1, :], jnp.where(is_second, route_ref[1:2, :], 0.0))
     earlier = (iota((tokens, tokens), 0) < iota((tokens, tokens), 1)).astype(F32).astype(BF16)
-    before = dot(named, earlier).astype(BF16)
-    slots = experts * capacity
-    slot = iota((slots, experts), 0)
-    owner = iota((slots, experts), 1) * capacity
-    spread = ((slot >= owner) & (slot < owner + capacity)).astype(F32).astype(BF16)
-    rank = (iota((slots, tokens), 0) % capacity).astype(F32)
-    chosen = (dot(spread, named) > 0.5) & (dot(spread, before) == rank)
-    mixing[...] = jnp.where(chosen, dot(spread, weight.astype(BF16)), 0.0).astype(BF16)
-    chosen = jnp.where(chosen, 1.0, 0.0).astype(BF16)
-
+    before = dot(named, earlier)
+    info[line] = jnp.concatenate(
+        [
+            first_id.astype(F32),
+            jnp.sum(jnp.where(is_first, before, 0.0), axis=0, keepdims=True),
+            second_id.astype(F32),
+            jnp.sum(jnp.where(is_second, before, 0.0), axis=0, keepdims=True),
+            jnp.zeros((4, tokens), F32),
+        ],
+        axis=0,
+    )
     values = input_ref[...].astype(F32)
     scale = lax.rsqrt(jnp.mean(values * values, axis=-1, keepdims=True) + norm_eps)
-    normed[...] = (values * scale * expert_gain_ref[...].astype(F32)).astype(BF16)
+    values = (values * scale * as_row(expert_gain_ref)).astype(BF16)
+    normed[...] = values
+    raw[line] = values
     tile = min(width, 512)
-    for start in range(0, width, tile):
-        block = dot(chosen, normed[:, start : start + tile])
-        block = block.reshape(ep_size, experts_local, capacity, tile)
-        outgoing[:, :, :, start : start + tile] = block.astype(BF16)
-    arrived[mine, group] = outgoing[group]
+
+    half = experts_local * capacity
+    row = iota((2 * half, tokens), 0)
+    own_half = row < half
+    row_expert = jnp.where(own_half, row // capacity + group * experts_local, row // capacity + (pair - 1) * experts_local)
+    row_expert = row_expert.astype(F32)
+    row_rank = (row % capacity).astype(F32)
+
+    def pick(at):
+        told = info[at]
+        wanted = ((row_expert == told[0:1]) & (row_rank == told[1:2])) | (
+            (row_expert == told[2:3]) & (row_rank == told[3:4])
+        )
+        wanted = jnp.where(wanted, 1.0, 0.0).astype(BF16)
+        for start in range(0, width, tile):
+            block = dot(wanted, raw[at, :, start : start + tile])
+            block = block.reshape(2, experts_local, capacity, tile).astype(BF16)
+            arrived[mine, 2 * at + pair_of, :, :, start : start + tile] = block[0]
+            crossing[at, :, :, start : start + tile] = block[1]
+
+    pick(line)
 
     select = {}
     for head in range(heads):
@@ -203,6 +238,14 @@
         select[head] = picked.astype(F32)
         queries[head] = dot(query_ref[...], (select[head] * DH ** (-0.5)).astype(BF16)).astype(BF16)
 
+    slots = experts * capacity
+    slot = iota((slots, experts), 0)
+    owner = iota((slots, experts), 1) * capacity
+    spread = ((slot >= owner) & (slot < owner + capacity)).astype(F32).astype(BF16)
+    rank = (iota((slots, tokens), 0) % capacity).astype(F32)
+    chosen = (dot(spread, named) > 0.5) & (dot(spread, before.astype(BF16)) == rank)
+    mixing[...] = jnp.where(chosen, dot(spread, weight.astype(BF16)), 0.0).astype(BF16)
+
     pl.semaphore_wait(barrier, ep_size + 1)
 
     def chain_copy(step):
@@ -224,15 +267,27 @@
     def _():
         pair_copy(0).start()
 
-    def dispatch_copy(step):
-        to = (group + ep_size - 1 - step) % ep_size
-        return remote(
-            outgoing.at[to], arrived.at[mine, group], send_sem.at[to], arrive_sem.at[mine, group], to, tp
-        )
-
-    def dispatch(step, carry):
-        dispatch_copy(step).start()
-        return carry
+    def raw_copies(at, to, raw_sent, info_sent):
+        return (
+            remote(raw.at[at], raw.at[at], raw_sent.at[at], raw_recv.at[at], to, tp),
+            remote(info.at[at], info.at[at], info_sent.at[at], info_recv.at[at], to, tp),
+        )
+
+    def send_up(at):
+        @pl.when(line + 1 < lines)
+        def _():
+            for copy in raw_copies(at, upper, raw_up, info_up):
+                copy.start()
+
+    def send_down(at):
+        @pl.when(line > 0)
+        def _():
+            for copy in raw_copies(at, lower, raw_down, info_down):
+                copy.start()
+
+    def y_copy(at):
+        block = 2 * at + pair_of
+        return remote(crossing.at[at], arrived.at[mine, block], y_sem.at[at], arrive_sem.at[mine, block], pair, tp)
 
     def x_copy(source, block):
         return remote(source, arrived.at[mine, block], x_sem.at[block], arrive_sem.at[mine, block], group, x_peer)
@@ -250,13 +305,27 @@
         part = arrived.at[place_of, block]
         remote(part, part, core_sem.at[block], arrive_sem.at[place_of, block], group, x_peer).wait_recv()
 
-    x_copy(outgoing.at[group], group).start()
-    core_copy(outgoing.at[group], group).start()
-    lax.fori_loop(0, group, dispatch, 0)
+    def pass_on(block):
+        x_copy(arrived.at[mine, block], block).start()
+        core_copy(arrived.at[mine, block], block).start()
+
+    def cross(at):
+        block = 2 * at + 1 - pair_of
+        await_rows(mine, block)
+        pass_on(block)
+
+    def take(at):
+        pick(at)
+        pass_on(2 * at + pair_of)
+        y_copy(at).start()
+
+    pass_on(group)
+    y_copy(line).start()
+    send_down(line)
 
     @pl.when(chain_of == 0)
     def _():
-        lax.fori_loop(group, ep_size - 1, dispatch, 0)
+        send_up(line)
 
     row_of = iota((rows, rows), 0)
     column_of = iota((rows, rows), 1)
@@ -296,6 +365,41 @@
 
     lax.fori_loop(0, heads, first_visit, 0)
 
+    def exchange(step):
+        @pl.when(step == 1)
+        def _():
+            cross(line)
+
+        @pl.when(step > 2)
+        def _():
+            at = jnp.where(step % 2 == 1, line + step // 2, line - (step - 2) // 2)
+
+            @pl.when((at >= 0) & (at < lines))
+            def _():
+                cross(jnp.clip(at, 0, lines - 1))
+
+        @pl.when(step > 1)
+        def _():
+            at = jnp.where(step % 2 == 0, line + step // 2, line - step // 2)
+            at_in = jnp.clip(at, 0, lines - 1)
+
+            @pl.when((at >= 0) & (at < lines))
+            def _():
+                for copy in raw_copies(at_in, upper, raw_up, info_up):
+                    copy.wait_recv()
+
+            @pl.when((at > line) & (at < lines))
+            def _():
+                send_down(at_in)
+
+            @pl.when((at >= 0) & (at < line))
+            def _():
+                send_up(at_in)
+
+            @pl.when((at >= 0) & (at < lines))
+            def _():
+                take(at_in)
+
     def attend(step, carry):
         @pl.when(step <= chain_of)
         def _():
@@ -309,7 +413,11 @@
 
         @pl.when(step == chain_of)
         def _():
-            lax.fori_loop(group, ep_size - 1, dispatch, 0)
+            send_up(line)
+
+        @pl.when(line < lines - 1)
+        def _():
+            exchange(step)
 
         @pl.when(step <= place)
         def _():
@@ -328,16 +436,28 @@
 
             lax.fori_loop(0, heads, next_visit, 0)
 
-        block = (group + step) % ep_size
-        await_rows(mine, block)
-        x_copy(arrived.at[mine, block], block).start()
-        core_copy(arrived.at[mine, block], block).start()
+        @pl.when(line == lines - 1)
+        def _():
+            exchange(step)
+
         return carry
 
     lax.fori_loop(1, ep_size, attend, 0)
+    last = line - (ep_size - 1) // 2
+
+    def block_of(step):
+        index = step // 2
+        both = jnp.minimum(line, lines - 1 - line)
+        near = jnp.where(index % 2 == 0, line - index // 2 - 1, line + index // 2 + 1)
+        far = index - both + 1
+        far = jnp.where(line > lines - 1 - line, line - far, line + far)
+        at = jnp.where(index < 2 * both, near, far)
+        at = jnp.where(index < lines - 1, at, line)
+        side = jnp.where(index < lines - 1, (pair_of + step) % 2, (pair_of + step + 1) % 2)
+        return jnp.clip(at, 0, lines - 1) * 2 + side
 
     def forward(step):
-        block = (group + 1 + step) % ep_size
+        block = block_of(step)
         await_rows(slot_x, block)
         core2_copy(block).start()
 
@@ -368,9 +488,11 @@
     )
     mixer_core_copy.start()
 
+    ring = partial.shape[0]
+
     def core_sum_copy(step):
         return remote(
-            partial.at[step, pl.ds((1 - core_of) * 2, 2)],
+            partial.at[step % ring, pl.ds((1 - core_of) * 2, 2)],
             from_core.at[step],
             s1_sem.at[step],
             r1_sem.at[step],
@@ -380,25 +502,42 @@
 
     def x_sum_copy(step):
         return remote(
-            partial.at[step, slot_x], from_x.at[step], s2_sem.at[step], r2_sem.at[step], group, x_peer
+            partial.at[step % ring, slot_x], from_x.at[step], s2_sem.at[step], r2_sem.at[step], group, x_peer
         )
 
     def return_copy(step):
-        to = (group + 1 + step) % ep_size
+        to = block_of(step)
         return remote(
-            partial.at[step, mine], returned.at[group], s3_sem.at[to], r3_sem.at[group], to, tp
-        )
+            partial.at[step % ring, mine], returned.at[group], s3_sem.at[to], r3_sem.at[group], to, tp
+        )
+
+    def left(step):
+        core_sum_copy(step).wait_send()
+        x_sum_copy(step).wait_send()
+
+        @pl.when(step < ep_size - 1)
+        def _():
+            return_copy(step).wait_send()
 
     def work(step, carry):
         @pl.when(step < ep_size)
         def _():
+            @pl.when((step == 1) & (last >= 0))
+            def _():
+                cross(jnp.maximum(last, 0))
+
             @pl.when(step + 1 < ep_size)
             def _():
                 forward(step + 1)
 
-            block = (group + 1 + step) % ep_size
+            block = block_of(step)
             await_rows(slot_core, block)
             await_rows(slot_diagonal, block)
+
+            @pl.when(step >= ring)
+            def _():
+                left(jnp.maximum(step - ring, 0))
+
             for expert in range(experts_local):
                 piece = joined(arrived[:, block, expert])
                 gate_proj = dot(piece, gate[expert])
@@ -407,7 +546,7 @@
                 for start in range(0, width, tile):
                     part = dot(hidden, down[expert, :, start : start + tile])
                     part = part.reshape(4, capacity, tile).astype(BF16)
-                    partial[step, :, expert, :, start : start + tile] = part
+                    partial[step % ring, :, expert, :, start : start + tile] = part
             core_sum_copy(step).start()
 
         @pl.when((step >= 1) & (step <= ep_size))
@@ -416,10 +555,10 @@
             core_sum_copy(past).wait_recv()
             for slot_of, x_at in ((slot_x, 1 - x_of), (mine, x_of)):
                 for expert in range(experts_local):
-                    total = partial[past, slot_of, expert].astype(F32) + from_core[
+                    total = partial[past % ring, slot_of, expert].astype(F32) + from_core[
                         past, x_at, expert
                     ].astype(F32)
-                    partial[past, slot_of, expert] = total.astype(BF16)
+                    partial[past % ring, slot_of, expert] = total.astype(BF16)
             x_sum_copy(past).start()
 
         @pl.when(step == ep_size - 1)
@@ -440,8 +579,8 @@
             past = step - 2
             x_sum_copy(past).wait_recv()
             for expert in range(experts_local):
-                total = partial[past, mine, expert].astype(F32) + from_x[past, expert].astype(F32)
-                partial[past, mine, expert] = total.astype(BF16)
+                total = partial[past % ring, mine, expert].astype(F32) + from_x[past, expert].astype(F32)
+                partial[past % ring, mine, expert] = total.astype(BF16)
 
             @pl.when(past < ep_size - 1)
             def _():
@@ -450,12 +589,12 @@
         return carry
 
     lax.fori_loop(0, ep_size + 2, work, 0)
-    returned[group] = partial[ep_size - 1, mine]
+    returned[group] = partial[(ep_size - 1) % ring, mine]
 
     mixer_x_copy.wait_recv()
     total = projected[mine].astype(F32) + mixer_x[...].astype(F32)
     scale = lax.rsqrt(jnp.mean(total * total, axis=-1, keepdims=True) + norm_eps)
-    mixer_out_ref[...] = (total * scale * mixer_gain_ref[...].astype(F32)).astype(BF16)
+    mixer_out_ref[...] = (total * scale * as_row(mixer_gain_ref)).astype(BF16)
 
     def await_return(step, carry):
         block = (group + 1 + step) % ep_size
@@ -492,24 +631,50 @@
 
     lax.fori_loop(1, chain_of + 1, pair_done, 0)
 
-    def sent(step, carry):
-        dispatch_copy(step).wait_send()
-        return_copy(step).wait_send()
+    @pl.when(line + 1 < lines)
+    def _():
+        def done(at, carry):
+            for copy in raw_copies(at, upper, raw_up, info_up):
+                copy.wait_send()
+            return carry
+
+        lax.fori_loop(0, line + 1, done, 0)
+
+    @pl.when(line > 0)
+    def _():
+        def done(at, carry):
+            for copy in raw_copies(at, lower, raw_down, info_down):
+                copy.wait_send()
+            return carry
+
+        lax.fori_loop(line, lines, done, 0)
+
+    def crossed(at, carry):
+        y_copy(at).wait_send()
         return carry
 
-    lax.fori_loop(0, ep_size - 1, sent, 0)
+    lax.fori_loop(0, lines, crossed, 0)
 
     def forwarded(block, carry):
         x_copy(arrived.at[mine, block], block).wait_send()
         core_copy(arrived.at[mine, block], block).wait_send()
         core2_copy(block).wait_send()
-        core_sum_copy(block).wait_send()
-        x_sum_copy(block).wait_send()
         return carry
 
     lax.fori_loop(0, ep_size, forwarded, 0)
+
+    def summed_up(step, carry):
+        left(step)
+        return carry
+
+    lax.fori_loop(ep_size - ring, ep_size, summed_up, 0)
     mixer_core_copy.wait_send()
     mixer_x_copy.wait_send()
+
+
+def hand_over_kernel(mixer_ref, expert_ref, mixer_out_ref, expert_out_ref):
+    mixer_out_ref[...] = mixer_ref[...]
+    expert_out_ref[...] = expert_ref[...]
 
 
 def on_device(
@@ -543,12 +708,13 @@
     parts = -(-rows // (2 * kv_width))
     block_rows = rows + 8 * (parts + parts % 2)
     share = rows // tp_size
+    lines = ep_size // 2
     cfg = (ep_size, experts_local, capacity, heads, kv_heads)
     piece = (experts_local, capacity, width)
     vmem = pl.BlockSpec(memory_space=pltpu.VMEM)
     hbm = pl.BlockSpec(memory_space=pl.ANY)
     dma = pltpu.SemaphoreType.DMA
-    return pl.pallas_call(
+    results = pl.pallas_call(
         functools.partial(layer_kernel, cfg),
         out_shape=(
             jax.ShapeDtypeStruct((share, width), BF16),
@@ -558,8 +724,10 @@
         out_specs=(vmem, vmem),
         scratch_shapes=[
             pltpu.VMEM((tp_size, ep_size) + piece, BF16),
-            pltpu.VMEM((ep_size,) + piece, BF16),
-            pltpu.VMEM((ep_size, tp_size) + piece, BF16),
+            pltpu.VMEM((lines, tokens, width), BF16),
+            pltpu.VMEM((lines, 8, tokens), F32),
+            pltpu.VMEM((lines,) + piece, BF16),
+            pltpu.VMEM((min(ep_size, 8), tp_size) + piece, BF16),
             pltpu.VMEM((ep_size, 2) + piece, BF16),
             pltpu.VMEM((ep_size,) + piece, BF16),
             pltpu.VMEM((ep_size,) + piece, BF16),
@@ -585,7 +753,14 @@
             dma((ep_size,)),
             dma((ep_size,)),
             dma((tp_size, ep_size)),
-            dma((ep_size,)),
+            dma((lines,)),
+            dma((lines,)),
+            dma((lines,)),
+            dma((lines,)),
+            dma((lines,)),
+            dma((lines,)),
+            dma((lines,)),
+
             dma((ep_size,)),
             dma((ep_size,)),
             dma((ep_size,)),
@@ -606,9 +781,9 @@
         key_rows,
         value_rows,
         break_bias.T,
-        mixer_gain.reshape(1, -1),
+        mixer_gain.reshape(-1, 128),
         expert_input,
-        expert_gain.reshape(1, -1),
+        expert_gain.reshape(-1, 128),
         route_ids.T,
         route_weights.T,
         mixer_weight,
@@ -619,6 +794,13 @@
         shared_up,
         shared_down,
     )
+    return pl.pallas_call(
+        hand_over_kernel,
+        out_shape=tuple(jax.ShapeDtypeStruct(result.shape, BF16) for result in results),
+        in_specs=[vmem] * 2,
+        out_specs=(vmem, vmem),
+        name="hand_over",
+    )(*results)
 
 
 def solution(mesh):

time: 156 us -> 131 us (0.84)
  the two profiles are of different devices: /device:TPU:12 before, /device:TPU:0 now
where the time goes in v1:
time: 131 us
  Pallas kernels  131 us (100%)
    pallas_call x1, Pallas kernels, on_device(): pl.pallas_call(functools.partial(layer_kernel, cfg), out_shape=(jax.Shape...  129 us

profile of v1, /device:TPU:0, one launch (start us, length us, event | category | flops | bytes accessed | tf_op | source)
XLA Modules:
  0.0 131.3 jit_solution(987641203255788372)
XLA Ops:
  0.6 128.5 %layer.1 = (bf16[96,2048]{1,0:T(8,128)(2,1)}, bf16[128,2048]{1,0:T(8,128)(2,1)}) custom-call(bf16[384,256]{1,0:T(8,128)(2,1)} %query_ref.1, bf16[384,128]{1,0:T(8,128)(2,1)} %key_ref.1, bf16[384,128]{1,0:T(8,128)(2,1)} %value_ref.1, bf16[4,384]{1,0:T(4,128)(2,1)} %bitcast.8, bf16[16,128]{1,0:T(8,128)(2,1)} %bitcast.5, bf16[128,2048]{1,0:T(8,128)(2,1)} %input_ref.1, ...), custom_call_target="tpu_custom_call" | custom-call | tf_op jit(solution)/shard_map/layer/pallas_call | solution.py:717
  129.2 2.1 %hand_over.1 = (bf16[96,2048]{1,0:T(8,128)(2,1)}, bf16[128,2048]{1,0:T(8,128)(2,1)}) custom-call(bf16[96,2048]{1,0:T(8,128)(2,1)} %get-tuple-element.4.mixer_ref, bf16[128,2048]{1,0:T(8,128)(2,1)} %get-tuple-element.5.expert_ref), custom_call_target="tpu_custom_call" | custom-call | tf_op jit(solution)/shard_map/hand_over/pallas_call | solution.py:797

commit v2 on v1

--- a/solution.py
+++ b/solution.py
@@ -400,58 +400,16 @@
             def _():
                 take(at_in)
 
-    def attend(step, carry):
-        @pl.when(step <= chain_of)
-        def _():
-            await_kv(base + jnp.maximum(place - 2 * step, 0))
-
-            @pl.when(chain_of + 1 < chains)
-            def _():
-                chain_copy(step).start()
-
-            pair_copy(step).start()
-
-        @pl.when(step == chain_of)
-        def _():
-            send_up(line)
-
-        @pl.when(line < lines - 1)
-        def _():
-            exchange(step)
-
-        @pl.when(step <= place)
-        def _():
-            block = base + jnp.maximum(place - step, 0)
-
-            @pl.when(step % 2 == 1)
-            def _():
-                await_kv(block)
-
-            def next_visit(head, carry):
-                summed, total = visit(block, head, False)
-                passed = later[head]
-                output[head] = output[head] + jnp.exp(passed) * summed
-                later[head] = passed + total
-                return carry
-
-            lax.fori_loop(0, heads, next_visit, 0)
-
-        @pl.when(line == lines - 1)
-        def _():
-            exchange(step)
-
-        return carry
-
-    lax.fori_loop(1, ep_size, attend, 0)
-    last = line - (ep_size - 1) // 2
-
     def block_of(step):
         index = step // 2
-        both = jnp.minimum(line, lines - 1 - line)
-        near = jnp.where(index % 2 == 0, line - index // 2 - 1, line + index // 2 + 1)
-        far = index - both + 1
-        far = jnp.where(line > lines - 1 - line, line - far, line + far)
-        at = jnp.where(index < 2 * both, near, far)
+        middle = lines // 2
+        lower_half = line < middle
+        depth = jnp.where(lower_half, middle - line, line - middle + 1)
+        turned = (index + depth) % middle
+        across = jnp.where(lower_half, middle + turned, middle - 1 - turned)
+        start = jnp.where(lower_half, 0, middle)
+        beside = start + (line - start + 1 + index) % middle
+        at = jnp.where(index < middle, across, beside)
         at = jnp.where(index < lines - 1, at, line)
         side = jnp.where(index < lines - 1, (pair_of + step) % 2, (pair_of + step + 1) % 2)
         return jnp.clip(at, 0, lines - 1) * 2 + side
@@ -460,33 +418,6 @@
         block = block_of(step)
         await_rows(slot_x, block)
         core2_copy(block).start()
-
-    forward(0)
-
-    attended = jnp.zeros((rows, heads * DH), F32)
-    for head in range(heads):
-        attended = attended + lax.dot_general(
-            output[head].astype(BF16),
-            select[head].astype(BF16),
-            (((1,), (1,)), ((), ())),
-            preferred_element_type=F32,
-        )
-    attended = attended.astype(BF16)
-    for load in loads:
-        load.wait()
-    share = projected.shape[1]
-    for to in range(projected.shape[0]):
-        for start in range(0, width, tile):
-            block = dot(attended[to * share : (to + 1) * share], mixer[:, start : start + tile])
-            projected[(to % 2) * 2 + to // 2, :, start : start + tile] = block.astype(BF16)
-
-    mixer_core_copy = remote(
-        projected.at[pl.ds((1 - core_of) * 2, 2)], mixer_core, mixer_sem.at[0], mixer_sem.at[1], group, core_peer
-    )
-    mixer_x_copy = remote(
-        projected.at[slot_x], mixer_x, mixer_sem.at[2], mixer_sem.at[3], group, x_peer
-    )
-    mixer_core_copy.start()
 
     ring = partial.shape[0]
 
@@ -519,47 +450,160 @@
         def _():
             return_copy(step).wait_send()
 
+    def expert_stage(step):
+        block = block_of(step)
+        await_rows(slot_core, block)
+        await_rows(slot_diagonal, block)
+
+        @pl.when(step >= ring)
+        def _():
+            left(jnp.maximum(step - ring, 0))
+
+        for expert in range(experts_local):
+            piece = joined(arrived[:, block, expert])
+            gate_proj = dot(piece, gate[expert])
+            up_proj = dot(piece, up[expert])
+            hidden = (jax.nn.silu(gate_proj) * up_proj).astype(BF16)
+            for start in range(0, width, tile):
+                part = dot(hidden, down[expert, :, start : start + tile])
+                part = part.reshape(4, capacity, tile).astype(BF16)
+                partial[step % ring, :, expert, :, start : start + tile] = part
+        core_sum_copy(step).start()
+
+    def core_stage(step):
+        core_sum_copy(step).wait_recv()
+        for slot_of, x_at in ((slot_x, 1 - x_of), (mine, x_of)):
+            for expert in range(experts_local):
+                total = partial[step % ring, slot_of, expert].astype(F32) + from_core[
+                    step, x_at, expert
+                ].astype(F32)
+                partial[step % ring, slot_of, expert] = total.astype(BF16)
+        x_sum_copy(step).start()
+
+    def x_stage(step):
+        x_sum_copy(step).wait_recv()
+        for expert in range(experts_local):
+            total = partial[step % ring, mine, expert].astype(F32) + from_x[step, expert].astype(F32)
+            partial[step % ring, mine, expert] = total.astype(BF16)
+
+        @pl.when(step < ep_size - 1)
+        def _():
+            return_copy(step).start()
+
+    early = (line == lines - 1) & (ring == ep_size)
+    late_steps = jnp.where(early, ep_size - 2, ep_size)
+
+    def attend(step, carry):
+        @pl.when(step <= chain_of)
+        def _():
+            await_kv(base + jnp.maximum(place - 2 * step, 0))
+
+            @pl.when(chain_of + 1 < chains)
+            def _():
+                chain_copy(step).start()
+
+            pair_copy(step).start()
+
+        @pl.when(step == chain_of)
+        def _():
+            send_up(line)
+
+        @pl.when(line < lines - 1)
+        def _():
+            exchange(step)
+
+        @pl.when(step <= place)
+        def _():
+            block = base + jnp.maximum(place - step, 0)
+
+            @pl.when(step % 2 == 1)
+            def _():
+                await_kv(block)
+
+            def next_visit(head, carry):
+                summed, total = visit(block, head, False)
+                passed = later[head]
+                output[head] = output[head] + jnp.exp(passed) * summed
+                later[head] = passed + total
+                return carry
+
+            lax.fori_loop(0, heads, next_visit, 0)
+
+        @pl.when(step == 1)
+        def _():
+            for load in loads:
+                load.wait()
+
+        @pl.when(early & (step == 2))
+        def _():
+            core_stage(ep_size - 1)
+            forward(ep_size - 2)
+            expert_stage(ep_size - 2)
+
+        @pl.when(early & (step == 3))
+        def _():
+            core_stage(ep_size - 2)
+
+        @pl.when(line == lines - 1)
+        def _():
+            exchange(step)
+
+        @pl.when(early & (step == 1))
+        def _():
+            forward(ep_size - 1)
+            expert_stage(ep_size - 1)
+
+        return carry
+
+    lax.fori_loop(1, ep_size, attend, 0)
+    last = line - (ep_size - 1) // 2
+
+    forward(0)
+
+    attended = jnp.zeros((rows, heads * DH), F32)
+    for head in range(heads):
+        attended = attended + lax.dot_general(
+            output[head].astype(BF16),
+            select[head].astype(BF16),
+            (((1,), (1,)), ((), ())),
+            preferred_element_type=F32,
+        )
+    attended = attended.astype(BF16)
+    share = projected.shape[1]
+    for to in range(projected.shape[0]):
+        for start in range(0, width, tile):
+            block = dot(attended[to * share : (to + 1) * share], mixer[:, start : start + tile])
+            projected[(to % 2) * 2 + to // 2, :, start : start + tile] = block.astype(BF16)
+
+    mixer_core_copy = remote(
+        projected.at[pl.ds((1 - core_of) * 2, 2)], mixer_core, mixer_sem.at[0], mixer_sem.at[1], group, core_peer
+    )
+    mixer_x_copy = remote(
+        projected.at[slot_x], mixer_x, mixer_sem.at[2], mixer_sem.at[3], group, x_peer
+    )
+    mixer_core_copy.start()
+
     def work(step, carry):
-        @pl.when(step < ep_size)
+        @pl.when(step < late_steps)
         def _():
             @pl.when((step == 1) & (last >= 0))
             def _():
                 cross(jnp.maximum(last, 0))
 
-            @pl.when(step + 1 < ep_size)
+            @pl.when(step + 1 < late_steps)
             def _():
                 forward(step + 1)
 
-            block = block_of(step)
-            await_rows(slot_core, block)
-            await_rows(slot_diagonal, block)
-
-            @pl.when(step >= ring)
-            def _():
-                left(jnp.maximum(step - ring, 0))
-
-            for expert in range(experts_local):
-                piece = joined(arrived[:, block, expert])
-                gate_proj = dot(piece, gate[expert])
-                up_proj = dot(piece, up[expert])
-                hidden = (jax.nn.silu(gate_proj) * up_proj).astype(BF16)
-                for start in range(0, width, tile):
-                    part = dot(hidden, down[expert, :, start : start + tile])
-                    part = part.reshape(4, capacity, tile).astype(BF16)
-                    partial[step % ring, :, expert, :, start : start + tile] = part
-            core_sum_copy(step).start()
-
-        @pl.when((step >= 1) & (step <= ep_size))
-        def _():
-            past = step - 1
-            core_sum_copy(past).wait_recv()
-            for slot_of, x_at in ((slot_x, 1 - x_of), (mine, x_of)):
-                for expert in range(experts_local):
-                    total = partial[past % ring, slot_of, expert].astype(F32) + from_core[
-                        past, x_at, expert
-                    ].astype(F32)
-                    partial[past % ring, slot_of, expert] = total.astype(BF16)
-            x_sum_copy(past).start()
+            expert_stage(step)
+
+        @pl.when((step >= 1) & (step <= late_steps))
+        def _():
+            core_stage(step - 1)
+
+        @pl.when(early & (step == 0))
+        def _():
+            x_stage(ep_size - 2)
+            x_stage(ep_size - 1)
 
         @pl.when(step == ep_size - 1)
         def _():
@@ -574,17 +618,9 @@
             for start in range(0, width, tile):
                 shared_out[:, start : start + tile] = dot(hidden, shared_down[:, start : start + tile])
 
-        @pl.when(step >= 2)
-        def _():
-            past = step - 2
-            x_sum_copy(past).wait_recv()
-            for expert in range(experts_local):
-                total = partial[past % ring, mine, expert].astype(F32) + from_x[past, expert].astype(F32)
-                partial[past % ring, mine, expert] = total.astype(BF16)
-
-            @pl.when(past < ep_size - 1)
-            def _():
-                return_copy(past).start()
+        @pl.when((step >= 2) & (step < late_steps + 2))
+        def _():
+            x_stage(step - 2)
 
         return carry
 

time: 131 us -> 127 us (0.969); the launches traced: 131 us -> 125 us
  Pallas kernels: 131 us -> 125 us
    pallas_call x1, Pallas kernels: 129 us -> 123 us  [on_device(): pl.pallas_call(functools.partial(layer_kernel, cfg), out_shape=(jax.Shape...]
where the time goes in v2:
time: 127 us; the launch traced here: 125 us
  Pallas kernels  125 us (98%)
    pallas_call x1, Pallas kernels, on_device(): pl.pallas_call(functools.partial(layer_kernel, cfg), out_shape=(jax.Shape...  123 us

profile of v2, /device:TPU:0, one launch (start us, length us, event | category | flops | bytes accessed | tf_op | source)
XLA Modules:
  0.0 125.3 jit_solution(14555918598357355688)
XLA Ops:
  0.6 122.5 %layer.1 = (bf16[96,2048]{1,0:T(8,128)(2,1)}, bf16[128,2048]{1,0:T(8,128)(2,1)}) custom-call(bf16[384,256]{1,0:T(8,128)(2,1)} %query_ref.1, bf16[384,128]{1,0:T(8,128)(2,1)} %key_ref.1, bf16[384,128]{1,0:T(8,128)(2,1)} %value_ref.1, bf16[4,384]{1,0:T(4,128)(2,1)} %bitcast.8, bf16[16,128]{1,0:T(8,128)(2,1)} %bitcast.5, bf16[128,2048]{1,0:T(8,128)(2,1)} %input_ref.1, ...), custom_call_target="tpu_custom_call" | custom-call | tf_op jit(solution)/shard_map/layer/pallas_call | solution.py:753
  123.1 2.1 %hand_over.1 = (bf16[96,2048]{1,0:T(8,128)(2,1)}, bf16[128,2048]{1,0:T(8,128)(2,1)}) custom-call(bf16[96,2048]{1,0:T(8,128)(2,1)} %get-tuple-element.4.mixer_ref, bf16[128,2048]{1,0:T(8,128)(2,1)} %get-tuple-element.5.expert_ref), custom_call_target="tpu_custom_call" | custom-call | tf_op jit(solution)/shard_map/hand_over/pallas_call | solution.py:833

commit v3 on v2

--- a/solution.py
+++ b/solution.py
@@ -365,7 +365,7 @@
 
     lax.fori_loop(0, heads, first_visit, 0)
 
-    def exchange(step):
+    def cross_before(step):
         @pl.when(step == 1)
         def _():
             cross(line)
@@ -378,6 +378,7 @@
             def _():
                 cross(jnp.clip(at, 0, lines - 1))
 
+    def take_next(step):
         @pl.when(step > 1)
         def _():
             at = jnp.where(step % 2 == 0, line + step // 2, line - step // 2)
@@ -399,6 +400,13 @@
             @pl.when((at >= 0) & (at < lines))
             def _():
                 take(at_in)
+
+    roomy = partial.shape[0] == ep_size
+    is_last = (line == lines - 1) & roomy
+    is_first_line = (line == 0) & roomy
+    early = is_last | is_first_line
+    own_step = jnp.where(is_first_line, ep_size - 2, ep_size - 1)
+    late_steps = jnp.where(is_last, ep_size - 2, jnp.where(is_first_line, ep_size - 1, ep_size))
 
     def block_of(step):
         index = step // 2
@@ -411,7 +419,8 @@
         beside = start + (line - start + 1 + index) % middle
         at = jnp.where(index < middle, across, beside)
         at = jnp.where(index < lines - 1, at, line)
-        side = jnp.where(index < lines - 1, (pair_of + step) % 2, (pair_of + step + 1) % 2)
+        last_side = jnp.where(step == own_step, pair_of, 1 - pair_of)
+        side = jnp.where(index < lines - 1, (pair_of + step) % 2, last_side)
         return jnp.clip(at, 0, lines - 1) * 2 + side
 
     def forward(step):
@@ -446,7 +455,7 @@
         core_sum_copy(step).wait_send()
         x_sum_copy(step).wait_send()
 
-        @pl.when(step < ep_size - 1)
+        @pl.when(step != own_step)
         def _():
             return_copy(step).wait_send()
 
@@ -486,14 +495,18 @@
             total = partial[step % ring, mine, expert].astype(F32) + from_x[step, expert].astype(F32)
             partial[step % ring, mine, expert] = total.astype(BF16)
 
-        @pl.when(step < ep_size - 1)
+        @pl.when(step != own_step)
         def _():
             return_copy(step).start()
 
-    early = (line == lines - 1) & (ring == ep_size)
-    late_steps = jnp.where(early, ep_size - 2, ep_size)
+    def early_step(step):
+        return jnp.where(is_last & (step == 2), ep_size - 2, ep_size - 1)
 
     def attend(step, carry):
+        @pl.when((is_last & (step == 2)) | (early & (step == 3)))
+        def _():
+            core_stage(early_step(step - 1))
+
         @pl.when(step <= chain_of)
         def _():
             await_kv(base + jnp.maximum(place - 2 * step, 0))
@@ -508,9 +521,15 @@
         def _():
             send_up(line)
 
-        @pl.when(line < lines - 1)
-        def _():
-            exchange(step)
+        @pl.when(line == lines // 2)
+        def _():
+            take_next(step)
+            cross_before(step)
+
+        @pl.when((line < lines - 1) & (line != lines // 2))
+        def _():
+            cross_before(step)
+            take_next(step)
 
         @pl.when(step <= place)
         def _():
@@ -534,24 +553,16 @@
             for load in loads:
                 load.wait()
 
-        @pl.when(early & (step == 2))
-        def _():
-            core_stage(ep_size - 1)
-            forward(ep_size - 2)
-            expert_stage(ep_size - 2)
-
-        @pl.when(early & (step == 3))
-        def _():
-            core_stage(ep_size - 2)
-
         @pl.when(line == lines - 1)
         def _():
-            exchange(step)
-
-        @pl.when(early & (step == 1))
-        def _():
-            forward(ep_size - 1)
-            expert_stage(ep_size - 1)
+            cross_before(step)
+            take_next(step)
+
+        @pl.when((is_last & (step == 1)) | (early & (step == 2)))
+        def _():
+            soon = early_step(step)
+            forward(soon)
+            expert_stage(soon)
 
         return carry
 
@@ -600,10 +611,9 @@
         def _():
             core_stage(step - 1)
 
-        @pl.when(early & (step == 0))
-        def _():
-            x_stage(ep_size - 2)
-            x_stage(ep_size - 1)
+        @pl.when((is_last & (step == 0)) | (early & (step == 1)))
+        def _():
+            x_stage(jnp.where(is_last & (step == 0), ep_size - 2, ep_size - 1))
 
         @pl.when(step == ep_size - 1)
         def _():
@@ -625,7 +635,7 @@
         return carry
 
     lax.fori_loop(0, ep_size + 2, work, 0)
-    returned[group] = partial[(ep_size - 1) % ring, mine]
+    returned[group] = partial[own_step % ring, mine]
 
     mixer_x_copy.wait_recv()
     total = projected[mine].astype(F32) + mixer_x[...].astype(F32)

time: 127 us -> 125 us (0.984)
  Pallas kernels: 125 us -> 122 us
    pallas_call x1, Pallas kernels: 123 us -> 120 us  [on_device(): pl.pallas_call(functools.partial(layer_kernel, cfg), out_shape=(jax.Shape...]
where the time goes in v3:
time: 125 us; the launch traced here: 122 us
  Pallas kernels  122 us (98%)
    pallas_call x1, Pallas kernels, on_device(): pl.pallas_call(functools.partial(layer_kernel, cfg), out_shape=(jax.Shape...  120 us

profile of v3, /device:TPU:0, one launch (start us, length us, event | category | flops | bytes accessed | tf_op | source)
XLA Modules:
  0.0 122.5 jit_solution(13767278561455465853)
XLA Ops:
  0.6 119.7 %layer.1 = (bf16[96,2048]{1,0:T(8,128)(2,1)}, bf16[128,2048]{1,0:T(8,128)(2,1)}) custom-call(bf16[384,256]{1,0:T(8,128)(2,1)} %query_ref.1, bf16[384,128]{1,0:T(8,128)(2,1)} %key_ref.1, bf16[384,128]{1,0:T(8,128)(2,1)} %value_ref.1, bf16[4,384]{1,0:T(4,128)(2,1)} %bitcast.8, bf16[16,128]{1,0:T(8,128)(2,1)} %bitcast.5, bf16[128,2048]{1,0:T(8,128)(2,1)} %input_ref.1, ...), custom_call_target="tpu_custom_call" | custom-call | tf_op jit(solution)/shard_map/layer/pallas_call | solution.py:763
  120.4 2.1 %hand_over.1 = (bf16[96,2048]{1,0:T(8,128)(2,1)}, bf16[128,2048]{1,0:T(8,128)(2,1)}) custom-call(bf16[96,2048]{1,0:T(8,128)(2,1)} %get-tuple-element.4.mixer_ref, bf16[128,2048]{1,0:T(8,128)(2,1)} %get-tuple-element.5.expert_ref), custom_call_target="tpu_custom_call" | custom-call | tf_op jit(solution)/shard_map/hand_over/pallas_call | solution.py:843
